TPU v7x, 32 devices: a whole 2x2x4 slice. The times are simulated.
32 devices in a mesh: kv: 4 (over y, x), tp: 8 (over z, core).
Axes of the slice: x: 2, y: 2, z: 4, core: 2. Of those that a mesh axis runs over, the one named last changes fastest.
Arguments:
- tokens: bfloat16 [3, 4096], P(None, ('kv', 'tp')), may hold values from -40 to 40
- lengths: int32 [3], replicated, may hold values from 1 to 8192, as said below
- attn_gain: float32 [4096], P(('kv', 'tp')), may hold values from 0.1 to 1.9
- w_query: bfloat16 [4096, 2048], P('kv', 'tp'), may hold values from -0.09375 to 0.09375
- w_key: bfloat16 [4096, 128], P('kv'), may hold values from -0.09375 to 0.09375
- w_value: bfloat16 [4096, 128], P('kv'), may hold values from -0.09375 to 0.09375
- w_forget: bfloat16 [4096, 32], replicated, may hold values from -0.09375 to 0.09375
- forget_bias: float32 [32], replicated, may hold values from -4 to 0
- cache_keys: bfloat16 [3, 128, 8192], P(None, None, ('kv', 'tp')), may hold values from -320 to 320
- cache_values: bfloat16 [3, 128, 8192], P(None, None, ('kv', 'tp')), may hold values from -6 to 6
- cache_decay: float32 [3, 32, 8192], P(None, None, ('kv', 'tp')), may hold values from -1028 to 0, as said below
- out_gain: float32 [2048], replicated, may hold values from 0.1 to 1.9
- w_out: bfloat16 [2048, 4096], P('tp', 'kv'), may hold values from -0.125 to 0.125
- mlp_gain: float32 [4096], P(('kv', 'tp')), may hold values from 0.1 to 1.9
- w_gate: bfloat16 [4096, 11264], P('kv', 'tp'), may hold values from -0.09375 to 0.09375
- w_up: bfloat16 [4096, 11264], P('kv', 'tp'), may hold values from -0.09375 to 0.09375
- w_down: bfloat16 [11264, 4096], P('tp', 'kv'), may hold values from -0.0546875 to 0.0546875
Outputs:
- layer_out: bfloat16 [3, 4096], P(None, ('kv', 'tp'))
Inputs may be any that keep to these rules, and one draw needn't show every extreme that they name: Sequence b has lengths[b] live cache positions, 0 to lengths[b] - 1; some sequence has exactly 8192 in every draw. On live positions, cache_decay[b, h, j] is the sum of the log forget gates of sequence b and head h over positions j + 1 to lengths[b] - 1, so it is zero at the last live position and never rises toward earlier positions; it is zero beyond lengths[b].
All inputs are finite; a program needn't handle non-finite values.
Results may differ from a plain program's by a relative error of at most 0.013.
Values may be sent and summed in bfloat16 or wider, within the bound.
A program may use at most 64 MiB of HBM per device.

v0:
```python
import jax
import jax.numpy as jnp
from jax import lax
from jax.sharding import PartitionSpec as P

QUERY_HEAD_COUNT = 32
HD = 64
KV_HEADS = 2
epsilon = 1e-06
masked_score = -1e30


def spread_rows(share, gain):
    scaled = (share.astype(jnp.float32) * gain).astype(jnp.bfloat16)
    squares = jnp.sum(jnp.square(share.astype(jnp.float32)), axis=1)
    row_block = lax.all_gather(scaled, "tp", axis=1, tiled=True)
    square_total = lax.psum(squares, ("kv", "tp"))
    return (row_block, square_total)


def body(
    tokens,
    lengths,
    attn_gain,
    w_query,
    w_key,
    w_value,
    w_forget,
    forget_bias,
    cache_keys,
    cache_values,
    cache_decay,
    out_gain,
    w_out,
    mlp_gain,
    w_gate,
    w_up,
    w_down,
):
    full_width = tokens.shape[1] * lax.axis_size("kv") * lax.axis_size("tp")
    kv_index = lax.axis_index("kv")
    tp_index = lax.axis_index("tp")
    row_block, square_total = spread_rows(tokens, attn_gain)
    block_rows = row_block.shape[1]
    forget_rows = lax.dynamic_slice_in_dim(w_forget, kv_index * block_rows, block_rows, 0)
    query_part = jnp.dot(row_block, w_query, preferred_element_type=jnp.float32)
    key_part = jnp.dot(row_block, w_key, preferred_element_type=jnp.float32)
    value_part = jnp.dot(row_block, w_value, preferred_element_type=jnp.float32)
    forget_part = jnp.dot(row_block, forget_rows, preferred_element_type=jnp.float32)
    query_sum, key_sum, value_sum, forget_sum = lax.psum(
        (query_part, key_part, value_part, forget_part), "kv"
    )
    first_rms = lax.rsqrt(square_total / full_width + epsilon)[:, None]
    query_local = (query_sum * first_rms).astype(jnp.bfloat16)
    key_new = (key_sum * first_rms).astype(jnp.bfloat16)
    value_new = (value_sum * first_rms).astype(jnp.bfloat16)
    log_gate = jax.nn.log_sigmoid(forget_sum * first_rms + forget_bias)
    query_all = lax.all_gather(query_local, "tp", axis=1, tiled=True)
    batch_rows, key_dims, span = cache_keys.shape
    groups = QUERY_HEAD_COUNT // KV_HEADS
    score_scale = HD ** (-0.5)
    query_grouped = query_all.reshape(batch_rows, KV_HEADS, groups, HD)
    keys_grouped = cache_keys.reshape(batch_rows, KV_HEADS, HD, span)
    values_grouped = cache_values.reshape(batch_rows, KV_HEADS, HD, span)
    scores = jnp.einsum(
        "bkgd,bkdj->bkgj", query_grouped, keys_grouped, preferred_element_type=jnp.float32
    ).reshape(batch_rows, QUERY_HEAD_COUNT, span)
    scores = scores * score_scale + cache_decay + log_gate[:, :, None]
    first_slot = (kv_index * lax.axis_size("tp") + tp_index) * span
    token_positions = first_slot + lax.iota(jnp.int32, span)
    is_live = (token_positions[None, :] < lengths[:, None])[:, None, :]
    scores = jnp.where(is_live, scores, masked_score)
    own_score = (
        jnp.einsum(
            "inpo,ino->inp",
            query_grouped,
            key_new.reshape(batch_rows, KV_HEADS, HD),
            preferred_element_type=jnp.float32,
        ).reshape(batch_rows, QUERY_HEAD_COUNT)
        * score_scale
    )
    local_top = jnp.maximum(jnp.max(scores, axis=2), own_score)
    head_count = w_out.shape[0] // HD
    head_start = tp_index * head_count
    score_top = lax.pmax(local_top, ("kv", "tp"))
    weights = jnp.where(is_live, jnp.exp(scores - score_top[:, :, None]), 0.0)
    weight_total = jnp.sum(weights, axis=2)
    rounded = weights.astype(jnp.bfloat16).reshape(batch_rows, KV_HEADS, groups, span)
    value_sums = jnp.einsum(
        "bkgj,bkdj->bkgd", rounded, values_grouped, preferred_element_type=jnp.float32
    ).reshape(batch_rows, QUERY_HEAD_COUNT, HD)
    weight_total, value_sums = (weight_total, value_sums)
    weight_total, value_sums = (
        lax.psum_scatter(weight_total, "tp", scatter_dimension=1, tiled=True),
        lax.psum_scatter(value_sums, "tp", scatter_dimension=1, tiled=True),
    )
    weight_total, value_sums = lax.psum((weight_total, value_sums), "kv")
    score_top = lax.dynamic_slice_in_dim(score_top, head_start, head_count, 1)
    own_here = lax.dynamic_slice_in_dim(own_score, head_start, head_count, 1)
    new_values = jnp.repeat(value_new.reshape(batch_rows, KV_HEADS, HD), groups, axis=1)
    new_values = lax.dynamic_slice_in_dim(new_values, head_start, head_count, 1).astype(jnp.float32)
    own_weight = jnp.exp(own_here - score_top)
    heads_out = (value_sums + own_weight[:, :, None] * new_values) / (weight_total + own_weight)[
        :, :, None
    ]
    head_gains = lax.dynamic_slice_in_dim(out_gain, head_start * HD, head_count * HD, 0).reshape(
        head_count, HD
    )
    normed = (
        heads_out
        * lax.rsqrt(jnp.mean(jnp.square(heads_out), axis=2, keepdims=True) + epsilon)
        * head_gains
    )
    normed = normed.astype(jnp.bfloat16).reshape(batch_rows, head_count * HD)
    attn_part = jnp.dot(normed, w_out, preferred_element_type=jnp.float32)
    attn_share = lax.psum_scatter(attn_part, "tp", scatter_dimension=1, tiled=True)
    residual = (tokens.astype(jnp.float32) + attn_share).astype(jnp.bfloat16)
    mlp_block, mlp_squares = spread_rows(residual, mlp_gain)
    gate_part = jnp.dot(mlp_block, w_gate, preferred_element_type=jnp.float32)
    up_part = jnp.dot(mlp_block, w_up, preferred_element_type=jnp.float32)
    gate_sum, up_sum = lax.psum((gate_part, up_part), "kv")
    second_rms = lax.rsqrt(mlp_squares / full_width + epsilon)[:, None]
    hidden = (jax.nn.silu(gate_sum * second_rms) * (up_sum * second_rms)).astype(jnp.bfloat16)
    down_part = jnp.dot(hidden, w_down, preferred_element_type=jnp.float32)
    mlp_share = lax.psum_scatter(down_part, "tp", scatter_dimension=1, tiled=True)
    return (residual.astype(jnp.float32) + mlp_share).astype(jnp.bfloat16)


def solution(mesh):
    placed = (
        P(None, ("kv", "tp")),
        P(),
        P(("kv", "tp")),
        P("kv", "tp"),
        P("kv", None),
        P("kv", None),
        P(),
        P(),
        P(None, None, ("kv", "tp")),
        P(None, None, ("kv", "tp")),
        P(None, None, ("kv", "tp")),
        P(),
        P("tp", "kv"),
        P(("kv", "tp")),
        P("kv", "tp"),
        P("kv", "tp"),
        P("tp", "kv"),
    )
    return jax.shard_map(
        body, mesh=mesh, in_specs=placed, out_specs=P(None, ("kv", "tp")), check_vma=False
    )
```

profile of v0, /device:TPU:0, one launch (start us, length us, event | category | flops | bytes accessed | tf_op | source)
XLA Modules:
  0.0 321.7 jit_solution(4829693310829404246)
XLA Ops:
  6.5 0.9 dynamic_slice.19
  7.5 0.7 mul.150
  8.2 0.8 fusion.11
  8.9 42.0 %psum.71 = f32[3]{0:T(128)S(1)} all-reduce(f32[3]{0:T(128)S(1)} %get-tuple-element.23), channel_id=1, replica_groups=mesh['kv'=4,'tp'=8] {'kv','tp'}, use_global_device_ids=true, to_apply=%region_2.0 | all-reduce | flops 3 | bytes 24 | tf_op jit(solution)/shard_map/psum | solution.py:17
  51.0 10.6 %all_gather.9 = bf16[3,1024]{1,0:T(4,128)(2,1)S(1)} all-gather(bf16[3,128]{1,0:T(4,128)(2,1)S(1)} %get-tuple-element.24), channel_id=1, replica_groups=mesh['kv'=4,'tp'=8] {'tp'}, dimensions={1}, use_global_device_ids=true | all-gather | bytes 6912 | tf_op jit(solution)/shard_map/all_gather | solution.py:16
  61.5 1.7 fusion.25
  63.2 1.1 fusion.22
  64.3 1.2 fusion.21
  65.5 1.0 fusion.3
  66.5 9.9 %all-reduce.5 = (f32[3,256]{1,0:T(4,128)S(1)}, f32[3,32]{1,0:T(4,128)S(1)}, f32[3,128]{1,0:T(4,128)S(1)}) all-reduce(f32[3,256]{1,0:T(4,128)S(1)} %fusion.21, f32[3,32]{1,0:T(4,128)S(1)} %fusion.3, f32[3,128]{1,0:T(4,128)S(1)} %fusion.22), channel_id=1, replica_groups=mesh['kv'=4,'tp'=8] {'kv'}, use_global_device_ids=true, to_apply=%region_0.0 | all-reduce | flops 1248 | bytes 9984 | tf_op jit(solution)/shard_map/psum | solution.py:50
  76.4 0.1 multiply_convert_fusion.1
  76.5 0.1 reshape.90
  76.6 12.8 %all_gather.10 = bf16[3,2048]{1,0:T(4,128)(2,1)S(1)} all-gather(bf16[3,256]{1,0:T(4,128)(2,1)S(1)} %multiply_convert_fusion.1), channel_id=1, replica_groups=mesh['kv'=4,'tp'=8] {'tp'}, dimensions={1}, use_global_device_ids=true | all-gather | bytes 13824 | tf_op jit(solution)/shard_map/all_gather | solution.py:58
  89.4 0.1 reshape.78
  89.5 0.1 fusion.23
  89.6 0.1 mul.142
  89.7 1.1 convolution_multiply_fusion
  90.8 0.7 broadcast_compare_fusion
  91.5 0.7 fusion.16
  92.2 1.0 fusion
  93.2 0.1 select_reduce_fusion
  93.4 37.8 %pmax.7 = f32[3,32]{1,0:T(4,128)} all-reduce(f32[3,32]{1,0:T(4,128)S(1)} %max.17), channel_id=1, replica_groups=mesh['kv'=4,'tp'=8] {'kv','tp'}, use_global_device_ids=true, to_apply=%region_6.7 | all-reduce | flops 96 | bytes 768 | tf_op jit(solution)/shard_map/pmax | solution.py:85
  131.2 1.4 fusion.1
  132.6 1.2 dynamic-slice
  134.5 1.1 fusion.24
  135.6 27.4 %all-reduce.2 = (f32[3,32,64]{2,1,0:T(8,128)S(1)}, f32[3,32]{1,0:T(4,128)S(1)}) all-reduce(f32[3,32,64]{2,1,0:T(8,128)S(1)} %bitcast.42, f32[3,32]{1,0:T(4,128)} %get-tuple-element.21), channel_id=2, replica_groups=mesh['kv'=4,'tp'=8] {'tp'}, use_global_device_ids=true, to_apply=%region_7.8.clone | all-reduce | flops 6240 | bytes 49920
  163.0 0.1 constant_dynamic-slice_fusion
  163.1 16.6 %all-reduce.4 = (f32[3,4,64]{2,1,0:T(4,128)S(1)}, f32[3,4]{1,0:T(4,128)S(1)}, f32[3,128]{1,0:T(4,128)S(1)}) all-reduce(f32[3,4,64]{2,1,0:T(4,128)S(1)} %constant_dynamic-slice_fusion.1, f32[3,4]{1,0:T(4,128)S(1)} %constant_dynamic-slice_fusion, f32[3,128]{1,0:T(4,128)} %fusion.25), channel_id=1, replica_groups=mesh['kv'=4,'tp'=8] {'kv'}, use_global_device_ids=true, to_apply=%region_8.9 | all-reduce | flops 1164 | bytes 9312 | tf_op jit(solution)/shard_map/psum | solution.py:97
  179.7 0.7 multiply_convert_fusion.2
  180.4 0.1 reshape.84
  180.5 0.8 fusion.20
  181.2 0.2 multiply_reduce_fusion
  181.4 0.8 multiply_convert_fusion
  182.2 0.1 reshape.86
  182.3 1.1 convolution_bitcast_fusion.1
  183.5 27.8 %reduce-scatter.9.cloned.1.call-done = f32[128,3]{1,0:T(8,128)} async-done(((f32[1024,3]{1,0:T(8,128)}), f32[128,3]{1,0:T(8,128)}) %reduce-scatter.9.cloned.1.call-update) | async-done | bytes 1552
  211.3 0.9 copy.24
  212.2 0.8 fusion.14
  213.0 37.8 %psum.78 = f32[3]{0:T(128)S(1)} all-reduce(f32[3]{0:T(128)S(1)} %get-tuple-element.15), channel_id=1, replica_groups=mesh['kv'=4,'tp'=8] {'kv','tp'}, use_global_device_ids=true, to_apply=%region_17.18 | all-reduce | flops 3 | bytes 24 | tf_op jit(solution)/shard_map/psum | solution.py:17
  250.8 0.8 fusion.13
  251.6 11.4 %all_gather.11 = bf16[3,1024]{1,0:T(4,128)(2,1)S(1)} all-gather(bf16[3,128]{1,0:T(4,128)(2,1)S(1)} %fusion.13), channel_id=1, replica_groups=mesh['kv'=4,'tp'=8] {'tp'}, dimensions={1}, use_global_device_ids=true | all-gather | bytes 6912 | tf_op jit(solution)/shard_map/all_gather | solution.py:16
  263.0 0.5 fusion.27
  263.5 0.5 fusion.26
  264.0 16.7 %all-reduce.3 = (f32[3,1408]{1,0:T(4,128)S(1)}, f32[3,1408]{1,0:T(4,128)S(1)}) all-reduce(f32[3,1408]{1,0:T(4,128)S(1)} %fusion.27, f32[3,1408]{1,0:T(4,128)S(1)} %fusion.26), channel_id=1, replica_groups=mesh['kv'=4,'tp'=8] {'kv'}, use_global_device_ids=true, to_apply=%region_18.19 | all-reduce | flops 8448 | bytes 67584 | tf_op jit(solution)/shard_map/psum | solution.py:121
  280.7 3.8 %convolution_bitcast_fusion = f32[1024,3]{1,0:T(8,128)} fusion(bf16[1408,1024]{1,0:T(8,128)(2,1)} %param.33, f32[3,1408]{1,0:T(4,128)S(1)} %get-tuple-element.7, f32[3,1408]{1,0:T(4,128)S(1)} %get-tuple-element.8, f32[3]{0:T(128)S(1)} %add_rsqrt_fusion.1), kind=kOutput, calls=%fused_computation | convolution fusion | flops 8684544 | bytes 2929676
  284.5 28.8 %reduce-scatter.11.cloned.1.call-done = f32[128,3]{1,0:T(8,128)} async-done(((f32[1024,3]{1,0:T(8,128)}), f32[128,3]{1,0:T(8,128)}) %reduce-scatter.11.cloned.1.call-update) | async-done | bytes 1552
  313.3 0.9 copy.26
  314.2 0.6 fusion.15
  (25 shorter events, 0.2 us)
Async XLA Ops:
  6.5 256.5 %copy-start = (bf16[1024,1408]{1,0:T(8,128)(2,1)S(1)}, bf16[1024,1408]{1,0:T(8,128)(2,1)}, u32[]{:S(2)}) copy-start(bf16[1024,1408]{1,0:T(8,128)(2,1)} %param.32) | copy-start | bytes 8650756
  6.5 175.7 %copy-start.2 = (bf16[256,1024]{1,0:T(8,128)(2,1)S(1)}, bf16[256,1024]{1,0:T(8,128)(2,1)}, u32[]{:S(2)}) copy-start(bf16[256,1024]{1,0:T(8,128)(2,1)} %param.29) | copy-start | bytes 1572868
  6.5 204.8 %reduce-scatter.9.cloned.1.call-start = ((), (), s32[]{:S(2)}) async-start(), calls=%async_computation.2 | async-start | bytes 589824
  50.9 40.6 %copy-start.5 = (f32[3]{0:T(128)}, f32[3]{0:T(128)S(1)}, u32[]{:S(2)}) copy-start(f32[3]{0:T(128)S(1)} %add_rsqrt_fusion.2) | copy-start | bytes 40
  89.7 3.7 %copy-start.3 = (f32[3,32]{1,0:T(4,128)}, f32[3,32]{1,0:T(4,128)S(1)}, u32[]{:S(2)}) copy-start(f32[3,32]{1,0:T(4,128)S(1)} %mul.142) | copy-start | bytes 1156
  91.5 1.7 copy-start.4
  183.4 129.9 %reduce-scatter.11.cloned.1.call-start = ((), (), s32[]{:S(2)}) async-start(), calls=%async_computation.3 | async-start | bytes 589824
  250.8 12.7 %copy-start.1 = (bf16[1024,1408]{1,0:T(8,128)(2,1)S(1)}, bf16[1024,1408]{1,0:T(8,128)(2,1)}, u32[]{:S(2)}) copy-start(bf16[1024,1408]{1,0:T(8,128)(2,1)} %param.31) | copy-start | bytes 8650756
Sparse Core Ops, SparseCore 0:
  183.5 27.7 reduce-scatter.8
  284.6 28.6 reduce-scatter.10
where the time goes:
time: 323 us; the launch traced here: 322 us
  blocking collectives  223 us (69%)
  waiting for transfers between devices  56.7 us (18%)
  between operations  14.1 us (4%)
  matrix products  13.2 us (4%)
  other arithmetic  9.52 us (3%)
  local copies, waits for them, and re-layouts  5.19 us (2%)
    psum x2, blocking collectives, spread_rows(): square_total = lax.psum(squares, ('kv', 'tp'))  79.8 us
    unnamed x4, waiting for transfers between devices  56.7 us
    pmax x1, blocking collectives, body(): score_top = lax.pmax(local_top, ('kv', 'tp'))  37.8 us
    unnamed x1, blocking collectives  27.4 us
    all_gather x2, blocking collectives, spread_rows(): row_block = lax.all_gather(scaled, 'tp', axis=1, tiled=True)  22 us
    psum x1, blocking collectives, body(): gate_sum, up_sum = lax.psum((gate_part, up_part), 'kv')  16.7 us
    psum x1, blocking collectives, body(): weight_total, value_sums = lax.psum((weight_total, value_sums), 'kv')  16.6 us
    all_gather x1, blocking collectives, body(): query_all = lax.all_gather(query_local, 'tp', axis=1, tiled=True)  12.8 us
  transfers between devices with their start and end apart: 2, of which 2 were waited for; matrix products, arithmetic and copies ran while one was open for 0% of the time, Pallas kernels for 0%

commit v1 on v0

--- a/solution.py
+++ b/solution.py
@@ -14,7 +14,9 @@
     scaled = (share.astype(jnp.float32) * gain).astype(jnp.bfloat16)
     squares = jnp.sum(jnp.square(share.astype(jnp.float32)), axis=1)
     row_block = lax.all_gather(scaled, "tp", axis=1, tiled=True)
-    square_total = lax.psum(squares, ("kv", "tp"))
+    square_total = squares
+    for jj in ("tp", "kv"):
+        square_total = lax.psum(square_total, jj)
     return (row_block, square_total)
 
 

time: 323 us -> 271 us (0.84)
  blocking collectives: 223 us -> 170 us
    psum x2, blocking collectives: 79.8 us -> 31.9 us  [spread_rows(): square_total = lax.psum(square_total, jj)]
    all_gather x2, blocking collectives: 22 us -> 17 us  [spread_rows(): row_block = lax.all_gather(scaled, 'tp', axis=1, tiled=True)]
where the time goes in v1:
time: 271 us; the launch traced here: 270 us
  blocking collectives  170 us (63%)
  waiting for transfers between devices  57 us (21%)
  between operations  14.2 us (5%)
  matrix products  13.2 us (5%)
  other arithmetic  9.51 us (4%)
  local copies, waits for them, and re-layouts  5.19 us (2%)
    unnamed x4, waiting for transfers between devices  57 us
    pmax x1, blocking collectives, body(): score_top = lax.pmax(local_top, ('kv', 'tp'))  38.2 us
    psum x2, blocking collectives, spread_rows(): square_total = lax.psum(square_total, jj)  31.9 us
    unnamed x1, blocking collectives  27 us
    all_gather x2, blocking collectives, spread_rows(): row_block = lax.all_gather(scaled, 'tp', axis=1, tiled=True)  17 us
    psum x1, blocking collectives, body(): gate_sum, up_sum = lax.psum((gate_part, up_part), 'kv')  16.8 us
    psum x1, blocking collectives, body(): weight_total, value_sums = lax.psum((weight_total, value_sums), 'kv')  16.5 us
    all_gather x1, blocking collectives, body(): query_all = lax.all_gather(query_local, 'tp', axis=1, tiled=True)  12.8 us
  transfers between devices with their start and end apart: 2, of which 2 were waited for; matrix products, arithmetic and copies ran while one was open for 0% of the time, Pallas kernels for 0%

profile of v1, /device:TPU:0, one launch (start us, length us, event | category | flops | bytes accessed | tf_op | source)
XLA Modules:
  0.0 269.6 jit_solution(2129917216340552273)
XLA Ops:
  6.5 0.9 dynamic_slice.19
  7.5 0.7 mul.150
  8.2 0.8 fusion.11
  8.9 18.1 %psum.85 = f32[3]{0:T(128)S(1)} all-reduce(f32[3]{0:T(128)S(1)} %get-tuple-element.25), channel_id=1, replica_groups=mesh['kv'=4,'tp'=8] {'tp'}, use_global_device_ids=true, to_apply=%region_2.0 | all-reduce | flops 3 | bytes 24 | tf_op jit(solution)/shard_map/psum | solution.py:19
  27.0 8.4 %all_gather.9 = bf16[3,1024]{1,0:T(4,128)(2,1)S(1)} all-gather(bf16[3,128]{1,0:T(4,128)(2,1)S(1)} %get-tuple-element.26), channel_id=1, replica_groups=mesh['kv'=4,'tp'=8] {'tp'}, dimensions={1}, use_global_device_ids=true | all-gather | bytes 6912 | tf_op jit(solution)/shard_map/all_gather | solution.py:16
  35.5 1.7 fusion.25
  37.1 1.1 fusion.22
  38.2 1.2 fusion.21
  39.4 1.0 fusion.3
  40.4 10.2 %all-reduce.5 = (f32[3,256]{1,0:T(4,128)S(1)}, f32[3]{0:T(128)S(1)}, f32[3,32]{1,0:T(4,128)S(1)}, f32[3,128]{1,0:T(4,128)S(1)}) all-reduce(f32[3,256]{1,0:T(4,128)S(1)} %fusion.21, f32[3]{0:T(128)S(1)} %psum.85, f32[3,32]{1,0:T(4,128)S(1)} %fusion.3, f32[3,128]{1,0:T(4,128)S(1)} %fusion.22), channel_id=1, replica_groups=mesh['kv'=4,'tp'=8] {'kv'}, use_global_device_ids=true, to_apply=%region_0.0 | all-reduce | flops 1251 | bytes 10008 | tf_op jit(solution)/shard_map/psum | solution.py:52
  50.7 0.1 multiply_convert_fusion.1
  50.8 0.1 reshape.90
  50.9 12.8 %all_gather.10 = bf16[3,2048]{1,0:T(4,128)(2,1)S(1)} all-gather(bf16[3,256]{1,0:T(4,128)(2,1)S(1)} %multiply_convert_fusion.1), channel_id=1, replica_groups=mesh['kv'=4,'tp'=8] {'tp'}, dimensions={1}, use_global_device_ids=true | all-gather | bytes 13824 | tf_op jit(solution)/shard_map/all_gather | solution.py:60
  63.6 0.1 reshape.78
  63.7 0.1 fusion.23
  63.9 0.1 mul.142
  64.0 1.1 convolution_multiply_fusion
  65.0 0.7 broadcast_compare_fusion
  65.8 0.7 fusion.16
  66.5 1.0 fusion
  67.5 0.1 select_reduce_fusion
  67.6 38.2 %pmax.7 = f32[3,32]{1,0:T(4,128)} all-reduce(f32[3,32]{1,0:T(4,128)S(1)} %max.17), channel_id=1, replica_groups=mesh['kv'=4,'tp'=8] {'kv','tp'}, use_global_device_ids=true, to_apply=%region_7.8 | all-reduce | flops 96 | bytes 768 | tf_op jit(solution)/shard_map/pmax | solution.py:87
  105.9 1.4 fusion.1
  107.3 1.2 dynamic-slice
  109.2 1.1 fusion.24
  110.3 27.0 %all-reduce.2 = (f32[3,32,64]{2,1,0:T(8,128)S(1)}, f32[3,32]{1,0:T(4,128)S(1)}) all-reduce(f32[3,32,64]{2,1,0:T(8,128)S(1)} %bitcast.42, f32[3,32]{1,0:T(4,128)} %get-tuple-element.23), channel_id=2, replica_groups=mesh['kv'=4,'tp'=8] {'tp'}, use_global_device_ids=true, to_apply=%region_8.9.clone | all-reduce | flops 6240 | bytes 49920
  137.3 0.1 constant_dynamic-slice_fusion
  137.4 16.5 %all-reduce.4 = (f32[3,4,64]{2,1,0:T(4,128)S(1)}, f32[3,4]{1,0:T(4,128)S(1)}, f32[3,128]{1,0:T(4,128)S(1)}) all-reduce(f32[3,4,64]{2,1,0:T(4,128)S(1)} %constant_dynamic-slice_fusion.1, f32[3,4]{1,0:T(4,128)S(1)} %constant_dynamic-slice_fusion, f32[3,128]{1,0:T(4,128)} %fusion.25), channel_id=1, replica_groups=mesh['kv'=4,'tp'=8] {'kv'}, use_global_device_ids=true, to_apply=%region_9.10 | all-reduce | flops 1164 | bytes 9312 | tf_op jit(solution)/shard_map/psum | solution.py:99
  153.9 0.7 multiply_convert_fusion.2
  154.6 0.1 reshape.84
  154.7 0.7 fusion.20
  155.4 0.2 multiply_reduce_fusion
  155.6 0.8 multiply_convert_fusion
  156.4 0.1 reshape.86
  156.5 1.1 convolution_bitcast_fusion.1
  157.7 27.7 %reduce-scatter.9.cloned.1.call-done = f32[128,3]{1,0:T(8,128)} async-done(((f32[1024,3]{1,0:T(8,128)}), f32[128,3]{1,0:T(8,128)}) %reduce-scatter.9.cloned.1.call-update) | async-done | bytes 1552
  185.4 0.9 copy.24
  186.3 0.8 fusion.14
  187.1 13.8 %psum.93 = f32[3]{0:T(128)S(1)} all-reduce(f32[3]{0:T(128)S(1)} %get-tuple-element.17), channel_id=1, replica_groups=mesh['kv'=4,'tp'=8] {'tp'}, use_global_device_ids=true, to_apply=%region_18.19 | all-reduce | flops 3 | bytes 24 | tf_op jit(solution)/shard_map/psum | solution.py:19
  200.9 0.8 fusion.13
  201.7 8.6 %all_gather.11 = bf16[3,1024]{1,0:T(4,128)(2,1)S(1)} all-gather(bf16[3,128]{1,0:T(4,128)(2,1)S(1)} %fusion.13), channel_id=1, replica_groups=mesh['kv'=4,'tp'=8] {'tp'}, dimensions={1}, use_global_device_ids=true | all-gather | bytes 6912 | tf_op jit(solution)/shard_map/all_gather | solution.py:16
  210.3 0.5 fusion.27
  210.8 0.5 fusion.26
  211.3 16.8 %all-reduce.3 = (f32[3,1408]{1,0:T(4,128)S(1)}, f32[3,1408]{1,0:T(4,128)S(1)}, f32[3]{0:T(128)S(1)}) all-reduce(f32[3,1408]{1,0:T(4,128)S(1)} %fusion.27, f32[3,1408]{1,0:T(4,128)S(1)} %fusion.26, f32[3]{0:T(128)S(1)} %psum.93), channel_id=1, replica_groups=mesh['kv'=4,'tp'=8] {'kv'}, use_global_device_ids=true, to_apply=%region_20.21 | all-reduce | flops 8451 | bytes 67608 | tf_op jit(solution)/shard_map/psum | solution.py:123
  228.1 3.8 %convolution_bitcast_fusion = f32[1024,3]{1,0:T(8,128)} fusion(bf16[1408,1024]{1,0:T(8,128)(2,1)} %param.33, f32[3,1408]{1,0:T(4,128)S(1)} %get-tuple-element.7, f32[3,1408]{1,0:T(4,128)S(1)} %get-tuple-element.8, f32[3]{0:T(128)S(1)} %add_rsqrt_fusion.1), kind=kOutput, calls=%fused_computation | convolution fusion | flops 8684544 | bytes 2929676
  232.0 29.3 %reduce-scatter.11.cloned.1.call-done = f32[128,3]{1,0:T(8,128)} async-done(((f32[1024,3]{1,0:T(8,128)}), f32[128,3]{1,0:T(8,128)}) %reduce-scatter.11.cloned.1.call-update) | async-done | bytes 1552
  261.3 0.9 copy.26
  262.2 0.6 fusion.15
  (25 shorter events, 0.2 us)
Async XLA Ops:
  6.5 203.8 %copy-start = (bf16[1024,1408]{1,0:T(8,128)(2,1)S(1)}, bf16[1024,1408]{1,0:T(8,128)(2,1)}, u32[]{:S(2)}) copy-start(bf16[1024,1408]{1,0:T(8,128)(2,1)} %param.32) | copy-start | bytes 8650756
  6.5 149.9 %copy-start.2 = (bf16[256,1024]{1,0:T(8,128)(2,1)S(1)}, bf16[256,1024]{1,0:T(8,128)(2,1)}, u32[]{:S(2)}) copy-start(bf16[256,1024]{1,0:T(8,128)(2,1)} %param.29) | copy-start | bytes 1572868
  6.5 178.8 %reduce-scatter.9.cloned.1.call-start = ((), (), s32[]{:S(2)}) async-start(), calls=%async_computation.2 | async-start | bytes 589824
  50.6 15.1 %copy-start.5 = (f32[3]{0:T(128)}, f32[3]{0:T(128)S(1)}, u32[]{:S(2)}) copy-start(f32[3]{0:T(128)S(1)} %add_rsqrt_fusion.2) | copy-start | bytes 40
  64.0 3.7 %copy-start.3 = (f32[3,32]{1,0:T(4,128)}, f32[3,32]{1,0:T(4,128)S(1)}, u32[]{:S(2)}) copy-start(f32[3,32]{1,0:T(4,128)S(1)} %mul.142) | copy-start | bytes 1156
  65.8 1.7 copy-start.4
  157.6 103.7 %reduce-scatter.11.cloned.1.call-start = ((), (), s32[]{:S(2)}) async-start(), calls=%async_computation.3 | async-start | bytes 589824
  200.9 9.8 %copy-start.1 = (bf16[1024,1408]{1,0:T(8,128)(2,1)S(1)}, bf16[1024,1408]{1,0:T(8,128)(2,1)}, u32[]{:S(2)}) copy-start(bf16[1024,1408]{1,0:T(8,128)(2,1)} %param.31) | copy-start | bytes 8650756
Sparse Core Ops, SparseCore 0:
  157.7 27.5 reduce-scatter.8
  232.1 29.1 reduce-scatter.10
